TPU v7x, 32 devices: a whole 2x2x4 slice. The times are simulated.
32 devices in a mesh: sp: 16 (over z, y, x), tp: 2 (over core).
Axes of the slice: x: 2, y: 2, z: 4, core: 2. Of those that a mesh axis runs over, the one named last changes fastest.
Arguments:
- acceptor_signal: bfloat16 [2048, 1024], P('sp', 'tp'), may hold values from -6 to 6
- address_entries: bfloat16 [2048, 1024], P('sp', 'tp'), may hold values from -6 to 6
- payload_entries: bfloat16 [2048, 1024], P('sp', 'tp'), may hold values from -6 to 6
- fading_logits: float32 [2048, 1024], P('sp', 'tp'), may hold values from -12 to -2
- learning_rate_logits: float32 [2048, 1024], P('sp', 'tp'), may hold values from -10 to 4
- exit_switch_entries: bfloat16 [2048, 1024], P('sp', 'tp'), may hold values from -6 to 6
- extra_reward_weights: float32 [1024], P('tp'), may hold values from -0.3 to 0.3
- subspace_rescale_weights: float32 [1024], P('tp'), may hold values from 0.1 to 1.9
- timemix_exit_weights: bfloat16 [1024, 2048], P('tp'), may hold values from -0.1875 to 0.1875
- skip_stream_arriving: bfloat16 [2048, 2048], P(('sp', 'tp')), may hold values from -6 to 6
- pointwise_block_scaling: float32 [2048], replicated, may hold values from 0.1 to 1.9
- switch_projection: bfloat16 [2048, 5632], P('sp', 'tp'), may hold values from -0.125 to 0.125
- widening_projection: bfloat16 [2048, 5632], P('sp', 'tp'), may hold values from -0.125 to 0.125
- switch_filter_coefficients: float32 [3, 5632], P(None, 'tp'), may hold values from -3.5 to 3.5
- narrowing_projection: bfloat16 [5632, 2048], P('tp', 'sp'), may hold values from -0.078125 to 0.078125
Outputs:
- layer_out: bfloat16 [2048, 2048], P(('sp', 'tp'))
All inputs are finite; a program needn't handle non-finite values.
Results may differ from a plain program's by a relative error of at most 0.019.
Values may be sent and summed in bfloat16 or wider, within the bound.
A program may use at most 128 MiB of HBM per device.

v0:
```python
import jax
import jax.numpy as jnp
from jax import lax
from jax.sharding import PartitionSpec as P

SUBSPACE_WIDTH = 64
SPAN = 16
group_eps = 0.00064
norm_eps = 1e-06
highest = lax.Precision.HIGHEST


def carried_in(shard, axis, join, neutral):
    place = lax.axis_index(axis)
    gathered = jax.tree.map(
        lambda a, kind: lax.all_gather(a.astype(kind), axis), shard, (jnp.bfloat16, jnp.bfloat16)
    )
    state = jax.tree.map(lambda a, e: jnp.zeros_like(a) + jnp.asarray(e, a.dtype), shard, neutral)

    def one(lap, state):
        return join(
            state,
            jax.tree.map(
                lambda a, own: lax.dynamic_index_in_dim(a, lap, 0, False).astype(own.dtype),
                gathered,
                shard,
            ),
        )

    return lax.fori_loop(0, place, one, state)


def shifted(block, axis, distance):
    devices = range(lax.axis_size(axis))
    route = [(i - distance, i) for i in devices if i - distance in devices]
    return lax.ppermute(block, axis, route)


def by_heads(array):
    return array.astype(jnp.float32).reshape(array.shape[0], -1, SUBSPACE_WIDTH)


def mechanism_inputs(
    acceptor_signal, address_entries, payload_entries, fading_logits, learning_rate_logits
):
    acceptor_entries = by_heads(acceptor_signal)
    address_mapped = by_heads(address_entries)
    payload_mapped = by_heads(payload_entries)
    log_rate = -jax.nn.softplus(-fading_logits) - 0.5
    fading = by_heads(jnp.exp(-jnp.exp(log_rate)))
    erase_rate = by_heads(jax.nn.sigmoid(learning_rate_logits))
    length = jnp.sqrt(jnp.sum(address_mapped * address_mapped, axis=-1, keepdims=True))
    unit_key = address_mapped / jnp.maximum(length, 1.0)
    return (
        acceptor_entries,
        address_mapped,
        payload_mapped,
        fading,
        -unit_key,
        unit_key * erase_rate,
    )


def subspace_outcomes(
    acceptor_entries,
    address_mapped,
    payload_mapped,
    closing_memory,
    subspace_rescale_weights,
    extra_reward_weights,
    exit_switch_entries,
):
    centred = closing_memory - jnp.mean(closing_memory, axis=-1, keepdims=True)
    rescaled_arguments = centred * lax.rsqrt(
        jnp.mean(centred * centred, axis=-1, keepdims=True) + group_eps
    )
    scaling_fetch = subspace_rescale_weights.reshape(-1, SUBSPACE_WIDTH)
    extra_reward_fetch = extra_reward_weights.reshape(-1, SUBSPACE_WIDTH)
    present_extra_reward = (
        jnp.sum(acceptor_entries * address_mapped * extra_reward_fetch, axis=-1, keepdims=True)
        * payload_mapped
    )
    timemix_product = rescaled_arguments * scaling_fetch + present_extra_reward
    timemix_product = timemix_product.reshape(
        timemix_product.shape[0], -1
    ) * exit_switch_entries.astype(jnp.float32)
    return timemix_product.astype(jnp.bfloat16)


def compose(earlier, latter):
    mapping = jnp.einsum("...ij,...jk->...ik", earlier[0], latter[0], precision=highest)
    state = jnp.einsum("...ij,...jk->...ik", earlier[1], latter[0], precision=highest) + latter[1]
    return (mapping, state)


def span_step(carried, sublevel_arguments):
    state, mapping = carried
    acceptor_entries, address_mapped, payload_mapped, fading, erase_dir, erase_amt = (
        sublevel_arguments
    )
    along = jnp.einsum("bhij,bhj->bhi", state, erase_dir, precision=highest)
    map_along = jnp.einsum("bhij,bhj->bhi", mapping, erase_dir, precision=highest)
    state = (
        state * fading[:, :, None, :]
        + along[..., None] * erase_amt[:, :, None, :]
        + payload_mapped[..., None] * address_mapped[:, :, None, :]
    )
    mapping = mapping * fading[:, :, None, :] + map_along[..., None] * erase_amt[:, :, None, :]
    local_out = jnp.einsum("bhij,bhj->bhi", state, acceptor_entries, precision=highest)
    probe = jnp.einsum("bhij,bhj->bhi", mapping, acceptor_entries, precision=highest)
    return ((state, mapping), (local_out, probe))


def recurrence(sublevel_arguments):
    token_count, head_count = (sublevel_arguments[0].shape[0], sublevel_arguments[0].shape[1])
    blocks = token_count // SPAN

    def arrange(member):
        return jnp.moveaxis(member.reshape(blocks, SPAN, head_count, SUBSPACE_WIDTH), 1, 0)

    arranged = tuple((arrange(member) for member in sublevel_arguments))
    unit_map = jnp.eye(SUBSPACE_WIDTH, dtype=jnp.float32)
    zero_state = jnp.zeros((blocks, head_count, SUBSPACE_WIDTH, SUBSPACE_WIDTH), jnp.float32)
    start_maps = jnp.broadcast_to(unit_map, zero_state.shape)
    (block_states, block_maps), (local_out, probe) = lax.scan(
        span_step, (zero_state, start_maps), arranged
    )
    cum_maps, cum_states = lax.associative_scan(compose, (block_maps, block_states))
    head_unit = jnp.broadcast_to(unit_map, (head_count, SUBSPACE_WIDTH, SUBSPACE_WIDTH))
    head_zero = jnp.zeros((head_count, SUBSPACE_WIDTH, SUBSPACE_WIDTH), jnp.float32)
    _, incoming = carried_in((cum_maps[-1], cum_states[-1]), "sp", compose, (head_unit, head_zero))
    prior_maps = jnp.concatenate([head_unit[None], cum_maps[:-1]], axis=0)
    prior_states = jnp.concatenate([head_zero[None], cum_states[:-1]], axis=0)
    entry = jnp.einsum("hij,bhjk->bhik", incoming, prior_maps, precision=highest) + prior_states
    closing_memory = local_out + jnp.einsum("bhij,tbhj->tbhi", entry, probe, precision=highest)
    return jnp.moveaxis(closing_memory, 0, 1).reshape(token_count, head_count, SUBSPACE_WIDTH)


def body(
    acceptor_signal,
    address_entries,
    payload_entries,
    fading_logits,
    learning_rate_logits,
    exit_switch_entries,
    extra_reward_weights,
    subspace_rescale_weights,
    timemix_exit_weights,
    skip_stream_arriving,
    pointwise_block_scaling,
    switch_projection,
    widening_projection,
    switch_filter_coefficients,
    narrowing_projection,
):
    gate_full, up_full, down_full = (
        lax.all_gather(switch_projection, "sp", axis=0, tiled=True),
        lax.all_gather(widening_projection, "sp", axis=0, tiled=True),
        lax.all_gather(narrowing_projection, "sp", axis=1, tiled=True),
    )
    sublevel_arguments = mechanism_inputs(
        acceptor_signal, address_entries, payload_entries, fading_logits, learning_rate_logits
    )
    closing_memory = recurrence(sublevel_arguments)
    timemix_product = subspace_outcomes(
        sublevel_arguments[0],
        sublevel_arguments[1],
        sublevel_arguments[2],
        closing_memory,
        subspace_rescale_weights,
        extra_reward_weights,
        exit_switch_entries,
    )
    token_count = timemix_product.shape[0]
    picked = timemix_product
    attended = lax.psum_scatter(
        jnp.dot(picked, timemix_exit_weights, preferred_element_type=jnp.float32).astype(
            jnp.bfloat16
        ),
        "tp",
        scatter_dimension=0,
        tiled=True,
    ).astype(jnp.float32)
    hidden_res = skip_stream_arriving.astype(jnp.float32) + attended
    rescaled_arguments = (
        hidden_res
        * lax.rsqrt(jnp.mean(hidden_res * hidden_res, axis=-1, keepdims=True) + norm_eps)
        * pointwise_block_scaling
    )
    rescaled_arguments = rescaled_arguments.astype(jnp.bfloat16)
    all_rows = lax.all_gather(rescaled_arguments, "tp", axis=0, tiled=True)
    gate_acc = jnp.dot(all_rows, gate_full, preferred_element_type=jnp.float32)
    up_acc = jnp.dot(all_rows, up_full, preferred_element_type=jnp.float32)
    gate_pre = gate_acc.astype(jnp.bfloat16)
    up_part = up_acc.astype(jnp.bfloat16)
    taps = switch_filter_coefficients.shape[0]
    tail_rows = shifted(gate_pre[token_count - taps + 1 :], "sp", 1)
    extended = jnp.concatenate([tail_rows, gate_pre], axis=0).astype(jnp.float32)
    conv_out = jnp.zeros(gate_pre.shape, jnp.float32)
    for tap in range(taps):
        conv_out = conv_out + switch_filter_coefficients[tap] * extended[tap : tap + token_count]
    hidden = (jax.nn.silu(conv_out) * up_part.astype(jnp.float32)).astype(jnp.bfloat16)
    picked = hidden
    projected = lax.psum_scatter(
        jnp.dot(picked, down_full, preferred_element_type=jnp.float32).astype(jnp.bfloat16),
        "tp",
        scatter_dimension=0,
        tiled=True,
    ).astype(jnp.float32)
    return (hidden_res + projected).astype(jnp.bfloat16)


def solution(mesh):
    return jax.shard_map(
        body,
        mesh=mesh,
        in_specs=(
            P("sp", "tp"),
            P("sp", "tp"),
            P("sp", "tp"),
            P("sp", "tp"),
            P("sp", "tp"),
            P("sp", "tp"),
            P("tp"),
            P("tp"),
            P("tp", None),
            P(("sp", "tp"), None),
            P(),
            P("sp", "tp"),
            P("sp", "tp"),
            P(None, "tp"),
            P("tp", "sp"),
        ),
        out_specs=P(("sp", "tp"), None),
        check_vma=False,
    )
```

profile of v0, /device:TPU:0, one launch (start us, length us, event | category | flops | bytes accessed | tf_op | source)
XLA Modules:
  0.0 1192.7 jit_solution(1004884859613980477)
XLA Ops:
  23.3 418.0 %while.30 = (s32[]{:T(128)}, f32[8,8,64,64]{3,2,1,0:T(8,128)}, f32[8,8,64,64]{3,2,1,0:T(8,128)}, f32[16,8,8,64]{3,0,2,1:T(8,128)}, f32[16,8,8,64]{3,0,2,1:T(8,12...) while((s32[]{:T(128)}, f32[8,8,64,64]{3,2,1,0:T(8,128)}, ...), condition=%wide.region_2.3_spmd.clone, body=%wide.region_1.2_spmd.clone.sunk | while | flops 15204355 | bytes 25657612 | solution.py:125
  48.5 5.1 fusion.113
  74.8 5.1 fusion.113
  101.0 5.1 fusion.113
  127.2 5.1 fusion.113
  153.4 5.1 fusion.113
  452.4 9.2 pad.48
  463.5 9.2 pad.47
  478.5 16.6 %pad.50 = f32[8,8,64,64]{3,2,1,0:T(8,128)} pad(f32[4,8,64,64]{3,2,1,0:T(8,128)} %copy-done.6, f32[]{:T(128)} %constant.54.clone.1), padding=1_0_1x0_0_0x0_0_0x0_0_0 | pad | bytes 1572868 | tf_op jit(solution)/shard_map/pad | solution.py:128
  497.4 16.7 %pad.49 = f32[8,8,64,64]{3,2,1,0:T(8,128)} pad(f32[4,8,64,64]{3,2,1,0:T(8,128)} %pad_maximum_fusion.1, f32[]{:T(128)} %constant.54.clone.1), padding=0_1_1x0_0_0x0_0_0x0_0_0 | pad | bytes 1572868 | tf_op jit(solution)/shard_map/pad | solution.py:128
  518.8 5.9 pad.41
  525.8 5.9 pad.42
  533.4 11.1 pad.112
  546.2 16.6 %pad.67 = f32[7,8,64,64]{3,2,1,0:T(8,128)} pad(f32[4,8,64,64]{3,2,1,0:T(8,128)} %pad_maximum_fusion.1, f32[]{:T(128)} %constant.54.clone.1), padding=0_0_1x0_0_0x0_0_0x0_0_0 | pad | bytes 1441796 | tf_op jit(solution)/shard_map/slice | solution.py:133
  563.8 11.2 pad.44
  577.1 11.2 pad.43
  594.9 46.1 %all-gather.6.cloned.1.call-done = bf16[16,8,64,64]{3,2,1,0:T(8,128)(2,1)} async-done(((bf16[1,8,64,64]{3,2,1,0:T(8,128)(2,1)}), bf16[16,8,64,64]{3,2,1,0:T(8,128)(2,1)}) %all-gather.6.cloned.1.call-update) | async-done | bytes 1048592 | tf_op jit(solution)/shard_map/all_gather | solution.py:16
  654.4 39.6 %reduce-scatter.3.cloned.1.call-done = bf16[64,2048]{1,0:T(8,128)(2,1)} async-done(((bf16[128,2048]{1,0:T(8,128)(2,1)}), bf16[64,2048]{1,0:T(8,128)(2,1)}) %reduce-scatter.3.cloned.1.call-update) | async-done | bytes 262160 | tf_op jit(solution)/shard_map/reduce_scatter | solution.py:176
  698.4 140.8 %all-gather.10.cloned.1.call-done = bf16[2048,2816]{1,0:T(8,128)(2,1)} async-done(((bf16[128,2816]{1,0:T(8,128)(2,1)}), bf16[2048,2816]{1,0:T(8,128)(2,1)}) %all-gather.10.cloned.1.call-update) | async-done | bytes 11534352 | tf_op jit(solution)/shard_map/all_gather | solution.py:157
  839.1 6.0 convolution_convert_fusion.1
  851.0 130.4 %all-gather.12.cloned.1.call-done = bf16[2048,2816]{1,0:T(8,128)(2,1)} async-done(((bf16[128,2816]{1,0:T(8,128)(2,1)}), bf16[2048,2816]{1,0:T(8,128)(2,1)}) %all-gather.12.cloned.1.call-update) | async-done | bytes 11534352 | tf_op jit(solution)/shard_map/all_gather | solution.py:158
  981.4 182.8 %all-gather.14.cloned.1.call-done = bf16[2816,2048]{1,0:T(8,128)(2,1)} async-done(((bf16[2816,128]{1,0:T(8,128)(2,1)}), bf16[2816,2048]{1,0:T(8,128)(2,1)}) %all-gather.14.cloned.1.call-update) | async-done | bytes 11534352 | tf_op jit(solution)/shard_map/all_gather | solution.py:159
  1164.2 13.6 %convolution_convert_fusion.2 = bf16[128,2048]{1,0:T(8,128)(2,1)} fusion(bf16[2816,2048]{1,0:T(8,128)(2,1)} %all-gather.14.cloned.1.call-done, bf16[128,2048]{1,0:T(8,128)(2,1)S(1)} %all_gather.22, bf16[2048,2816]{1,0:T(8,128)(2,1)} %all-gather.12.cloned.1.call-done, f32[130,2816]{1,0:T(8,128)} %maximum_convert_fusion, f32[2816]{0:T(1024)S(1)} %get-tuple-element.188, ...), kind=kOutput, calls=%fused_computation.27 | convolution fusion | flops 2957737984 | bytes 28476416 | tf_op jit(solution)/shard_map/dot_general | solution.py:205
  1177.8 6.3 reduce-scatter.5.cloned.1.call-done
  (426 shorter events, 473.3 us)
Async XLA Ops:
  6.5 643.8 %copy-start = (bf16[512,2048]{1,0:T(8,128)(2,1)S(1)}, bf16[512,2048]{1,0:T(8,128)(2,1)}, u32[]{:S(2)}) copy-start(bf16[512,2048]{1,0:T(8,128)(2,1)} %param.27) | copy-start | bytes 6291460
  6.5 588.4 %all-gather.8.cloned.1.call-start = ((), (), s32[]{:S(2)}) async-start(), calls=%async_computation.3 | async-start | bytes 2228224 | tf_op jit(solution)/shard_map/all_gather | solution.py:16
  7.9 13.7 %copy-start.21 = (f32[64,64]{1,0:T(8,128)}, f32[64,64]{1,0:T(8,128)S(1)}, u32[]{:S(2)}) copy-start(f32[64,64]{1,0:T(8,128)S(1)} %fusion.61) | copy-start | bytes 49156
  48.5 10.0 copy-start.4
  74.8 10.0 copy-start.4
  101.0 10.0 copy-start.4
  127.2 10.0 copy-start.4
  153.4 10.0 copy-start.4
  179.6 10.0 copy-start.4
  450.7 10.9 slice-start
  478.5 16.6 %copy-start.17 = (f32[1,8,64,64]{3,2,1,0:T(8,128)S(1)}, f32[1,8,64,64]{3,2,1,0:T(8,128)}, u32[]{:S(2)}) copy-start(f32[1,8,64,64]{3,2,1,0:T(8,128)} %slice.129) | copy-start | bytes 393220
  515.8 125.2 %all-gather.6.cloned.1.call-start = ((), (), s32[]{:S(2)}) async-start(), calls=%async_computation.2 | async-start | bytes 2228224 | tf_op jit(solution)/shard_map/all_gather | solution.py:16
  546.1 147.8 %reduce-scatter.3.cloned.1.call-start = ((), (), s32[]{:S(2)}) async-start(), calls=%async_computation.4 | async-start | bytes 786432 | tf_op jit(solution)/shard_map/reduce_scatter | solution.py:176
  577.1 11.3 copy-start.26
  577.1 11.3 copy-start.16
  652.6 41.4 %copy-start.12 = (bf16[64,2048]{1,0:T(8,128)(2,1)S(1)}, bf16[64,2048]{1,0:T(8,128)(2,1)}, u32[]{:S(2)}) copy-start(bf16[64,2048]{1,0:T(8,128)(2,1)} %param.28) | copy-start | bytes 786436
  652.6 42.6 %copy-start.24 = (f32[2048]{0:T(1024)S(1)}, f32[2048]{0:T(1024)}, u32[]{:S(2)}) copy-start(f32[2048]{0:T(1024)} %param.29) | copy-start | bytes 24580
  652.6 186.6 %all-gather.10.cloned.1.call-start = ((), (), s32[]{:S(2)}) async-start(), calls=%async_computation.5 | async-start | bytes 12255232 | tf_op jit(solution)/shard_map/all_gather | solution.py:157
  653.2 328.2 %all-gather.12.cloned.1.call-start = ((), (), s32[]{:S(2)}) async-start(), calls=%async_computation.6 | async-start | bytes 12255232 | tf_op jit(solution)/shard_map/all_gather | solution.py:158
  653.7 510.5 %all-gather.14.cloned.1.call-start = ((), (), s32[]{:S(2)}) async-start(), calls=%async_computation.7 | async-start | bytes 12255232 | tf_op jit(solution)/shard_map/all_gather | solution.py:159
  654.3 529.8 %reduce-scatter.5.cloned.1.call-start = ((), (), s32[]{:S(2)}) async-start(), calls=%async_computation.8 | async-start | bytes 786432 | tf_op jit(solution)/shard_map/reduce_scatter | solution.py:204
  698.4 150.2 %copy-start.23 = (f32[3,2816]{1,0:T(4,128)S(1)}, f32[3,2816]{1,0:T(4,128)}, u32[]{:S(2)}) copy-start(f32[3,2816]{1,0:T(4,128)} %param.32) | copy-start | bytes 101380
  845.1 4.6 collective-permute-start
  1164.2 19.9 %copy-start.13 = (bf16[64,2048]{1,0:T(8,128)(2,1)S(1)}, bf16[64,2048]{1,0:T(8,128)(2,1)}, u32[]{:S(2)}) copy-start(bf16[64,2048]{1,0:T(8,128)(2,1)} %reduce-scatter.3.cloned.1.call-done) | copy-start | bytes 786436
  (72 other events, 321.6 us)
Sparse Core Ops, SparseCore 0:
  515.9 63.0 all-gather.7
  581.9 59.1 all-gather.5
  652.7 41.2 reduce-scatter.2
  696.6 142.5 all-gather.9
  841.7 139.5 all-gather.11
  983.9 180.2 all-gather.13
  1178.0 6.0 reduce-scatter.4
where the time goes:
time: 1210 us; the launch traced here: 1190 us
  waiting for transfers between devices  549 us (45%)
  matrix products  311 us (26%)
  local copies, waits for them, and re-layouts  248 us (20%)
  other arithmetic  64.1 us (5%)
  between operations  14.1 us (1%)
    all_gather x1, waiting for transfers between devices, body(): lax.all_gather(narrowing_projection, 'sp', axis=1, tiled=True)  183 us
    all_gather x1, waiting for transfers between devices, body(): lax.all_gather(switch_projection, 'sp', axis=0, tiled=True)  141 us
    all_gather x1, waiting for transfers between devices, body(): lax.all_gather(widening_projection, 'sp', axis=0, tiled=True)  130 us
    pad x8, local copies, waits for them, and re-layouts, recurrence(): lax.associative_scan(compose, (block_maps, block_states))  86 us
    dot_general x16, matrix products, span_step(): along = jnp.einsum('bhij,bhj->bhi', state, erase_dir, precision=highest)  79.9 us
    dot_general x16, matrix products, span_step(): jnp.einsum('bhij,bhj->bhi', state, acceptor_entries, precision=highest)  79 us
    dynamic_update_slice x32, local copies, waits for them, and re-layouts, recurrence(): lax.scan(span_step, (zero_state, start_maps), arranged)  57 us
    dot_general x16, matrix products, span_step(): jnp.einsum('bhij,bhj->bhi', mapping, erase_dir, precision=highest)  53.9 us
  transfers between devices with their start and end apart: 8, of which 7 were waited for; matrix products, arithmetic and copies ran while one was open for 7% of the time, Pallas kernels for 0%

commit v1 on v0

--- a/solution.py
+++ b/solution.py
@@ -8,6 +8,28 @@
 group_eps = 0.00064
 norm_eps = 1e-06
 highest = lax.Precision.HIGHEST
+
+
+def laid_out(parts, dim):
+    shape = list(parts.shape[1:])
+    shape[dim] *= parts.shape[0]
+    return jnp.moveaxis(parts, 0, dim).reshape(shape)
+
+
+def ring_gather(x, axis, dim):
+    size = lax.axis_size(axis)
+    pairs = [(i, (i + 1) % size) for i in range(size)]
+    back = [(b, a) for a, b in pairs]
+    lower, upper = ([], [])
+    for step in range(size - 1):
+        if step % 2 == 0:
+            lower.append(lax.ppermute(lower[-1] if lower else x, axis, pairs))
+        else:
+            upper.append(lax.ppermute(upper[-1] if upper else x, axis, back))
+    blocks = jnp.stack([*lower[::-1], x, *upper])
+    shift = lax.axis_index(axis) - len(lower)
+    blocks = blocks[(jnp.arange(size) - shift) % size]
+    return laid_out(blocks, dim)
 
 
 def carried_in(shard, axis, join, neutral):
@@ -156,7 +178,7 @@
     gate_full, up_full, down_full = (
         lax.all_gather(switch_projection, "sp", axis=0, tiled=True),
         lax.all_gather(widening_projection, "sp", axis=0, tiled=True),
-        lax.all_gather(narrowing_projection, "sp", axis=1, tiled=True),
+        ring_gather(narrowing_projection, "sp", 1),
     )
     sublevel_arguments = mechanism_inputs(
         acceptor_signal, address_entries, payload_entries, fading_logits, learning_rate_logits

time: 1210 us -> 1170 us (0.967)
  waiting for transfers between devices: 549 us -> 319 us
  starting transfers between devices: 3.68 us -> 138 us
  local copies, waits for them, and re-layouts: 248 us -> 297 us
    all_gather x1 -> x0, waiting for transfers between devices: 183 us -> none  [body(): lax.all_gather(narrowing_projection, 'sp', axis=1, tiled=True)]
    ppermute x0 -> x15, waiting for transfers between devices: none -> 178 us  [the longest x8 106 us: ring_gather(): lower.append(lax.ppermute(lower[-1] if lower else x, axis, pairs))]
    all_gather x1, waiting for transfers between devices: 141 us -> 0.01 us  [body(): lax.all_gather(switch_projection, 'sp', axis=0, tiled=True)]
    ppermute x0 -> x15, starting transfers between devices: none -> 136 us  [the longest x7 128 us: ring_gather(): upper.append(lax.ppermute(upper[-1] if upper else x, axis, back))]
    all_gather x1, waiting for transfers between devices: 130 us -> 87.5 us  [body(): lax.all_gather(widening_projection, 'sp', axis=0, tiled=True)]
    reduce_scatter x1, waiting for transfers between devices: 39.6 us -> 0.02 us  [body(): lax.psum_scatter(jnp.dot(picked, timemix_exit_weights, preferred_element_...]
    unnamed x49 -> x92, local copies, waits for them, and re-layouts: 14.9 us -> 35.6 us
    transpose x0 -> x1, local copies, waits for them, and re-layouts: none -> 15.1 us  [laid_out(): return jnp.moveaxis(parts, 0, dim).reshape(shape)]
  transfers between devices with their start and end apart: 8 -> 22, of which waited for: 7 -> 11; matrix products, arithmetic and copies ran while one was open for 7% -> 12% of each run, Pallas kernels for 0% -> 0%
where the time goes in v1:
time: 1170 us; the launch traced here: 1150 us
  waiting for transfers between devices  319 us (27%)
  matrix products  311 us (27%)
  local copies, waits for them, and re-layouts  297 us (25%)
  starting transfers between devices  138 us (12%)
  other arithmetic  63 us (5%)
  between operations  14.4 us (1%)
    ppermute x7, starting transfers between devices, ring_gather(): upper.append(lax.ppermute(upper[-1] if upper else x, axis, back))  128 us
    ppermute x8, waiting for transfers between devices, ring_gather(): lower.append(lax.ppermute(lower[-1] if lower else x, axis, pairs))  106 us
    all_gather x1, waiting for transfers between devices, body(): lax.all_gather(widening_projection, 'sp', axis=0, tiled=True)  87.5 us
    pad x8, local copies, waits for them, and re-layouts, recurrence(): lax.associative_scan(compose, (block_maps, block_states))  86 us
    dot_general x16, matrix products, span_step(): along = jnp.einsum('bhij,bhj->bhi', state, erase_dir, precision=highest)  79.9 us
    dot_general x16, matrix products, span_step(): jnp.einsum('bhij,bhj->bhi', state, acceptor_entries, precision=highest)  79 us
    ppermute x7, waiting for transfers between devices, ring_gather(): upper.append(lax.ppermute(upper[-1] if upper else x, axis, back))  71.5 us
    dynamic_update_slice x32, local copies, waits for them, and re-layouts, recurrence(): lax.scan(span_step, (zero_state, start_maps), arranged)  57.1 us
  transfers between devices with their start and end apart: 22, of which 11 were waited for; matrix products, arithmetic and copies ran while one was open for 12% of the time, Pallas kernels for 0%

profile of v1, /device:TPU:0, one launch (start us, length us, event | category | flops | bytes accessed | tf_op | source)
XLA Modules:
  0.0 1146.0 jit_solution(7805709490829501124)
XLA Ops:
  23.2 418.4 %while.30 = (s32[]{:T(128)}, f32[8,8,64,64]{3,2,1,0:T(8,128)}, f32[8,8,64,64]{3,2,1,0:T(8,128)}, f32[16,8,8,64]{3,0,2,1:T(8,128)}, f32[16,8,8,64]{3,0,2,1:T(8,12...) while((s32[]{:T(128)}, f32[8,8,64,64]{3,2,1,0:T(8,128)}, ...), condition=%wide.region_2.3_spmd.clone, body=%wide.region_1.2_spmd.clone.sunk | while | flops 15204355 | bytes 25657612 | solution.py:147
  462.0 9.2 pad.48
  477.1 16.7 %pad.50 = f32[8,8,64,64]{3,2,1,0:T(8,128)} pad(f32[4,8,64,64]{3,2,1,0:T(8,128)} %copy-done.6, f32[]{:T(128)} %constant.70.clone.1), padding=1_0_1x0_0_0x0_0_0x0_0_0 | pad | bytes 1572868 | tf_op jit(solution)/shard_map/pad | solution.py:150
  496.0 16.7 %pad.49 = f32[8,8,64,64]{3,2,1,0:T(8,128)} pad(f32[4,8,64,64]{3,2,1,0:T(8,128)} %pad_maximum_fusion.1, f32[]{:T(128)} %constant.70.clone.1), padding=0_1_1x0_0_0x0_0_0x0_0_0 | pad | bytes 1572868 | tf_op jit(solution)/shard_map/pad | solution.py:150
  531.9 11.2 pad.114
  544.8 16.6 %pad.68 = f32[7,8,64,64]{3,2,1,0:T(8,128)} pad(f32[4,8,64,64]{3,2,1,0:T(8,128)} %pad_maximum_fusion.1, f32[]{:T(128)} %constant.70.clone.1), padding=0_0_1x0_0_0x0_0_0x0_0_0 | pad | bytes 1441796 | tf_op jit(solution)/shard_map/slice | solution.py:155
  562.4 11.1 pad.44
  575.7 11.2 pad.43
  593.5 46.1 %all-gather.5.cloned.1.call-done = bf16[16,8,64,64]{3,2,1,0:T(8,128)(2,1)} async-done(((bf16[1,8,64,64]{3,2,1,0:T(8,128)(2,1)}), bf16[16,8,64,64]{3,2,1,0:T(8,128)(2,1)}) %all-gather.5.cloned.1.call-update) | async-done | bytes 1048592 | tf_op jit(solution)/shard_map/all_gather | solution.py:38
  655.4 49.9 %collective-permute-done.1 = bf16[2816,128]{1,0:T(8,128)(2,1)S(1)} collective-permute-done((bf16[2816,128]{1,0:T(8,128)(2,1)}, bf16[2816,128]{1,0:T(8,128)(2,1)S(1)}, u32[]{:S(2)}, u32[]{:S(2)}) %collective-permute-start.1) | collective-permute-done | bytes 720928 | tf_op jit(solution)/shard_map/ppermute | solution.py:26
  711.0 29.8 %collective-permute-done.2 = bf16[2816,128]{1,0:T(8,128)(2,1)S(1)} collective-permute-done((bf16[2816,128]{1,0:T(8,128)(2,1)S(1)}, bf16[2816,128]{1,0:T(8,128)(2,1)S(1)}, u32[]{:S(2)}, u32[]{:S(2)}) %collective-permute-start.2) | collective-permute-done | bytes 720928 | tf_op jit(solution)/shard_map/ppermute | solution.py:26
  741.6 18.5 %collective-permute-start.10 = (bf16[2816,128]{1,0:T(8,128)(2,1)S(1)}, bf16[2816,128]{1,0:T(8,128)(2,1)S(1)}, u32[]{:S(2)}, u32[]{:S(2)}) collective-permute-start(bf16[2816,128]{1,0:T(8,128)(2,1)S(1)} %collective-permute-done.9), channel_id=1, source_target_pairs={{2,0},{4,2},{6,4},{8,6},{10,8},{12,10},{14,12},{16,14},{18,16},{20... | collective-permute-start | bytes 2162696 | tf_op jit(solution)/shard_map/ppermute | solution.py:28
  760.1 21.9 %collective-permute-done.3 = bf16[2816,128]{1,0:T(8,128)(2,1)S(1)} collective-permute-done((bf16[2816,128]{1,0:T(8,128)(2,1)S(1)}, bf16[2816,128]{1,0:T(8,128)(2,1)S(1)}, u32[]{:S(2)}, u32[]{:S(2)}) %collective-permute-start.3) | collective-permute-done | bytes 720928 | tf_op jit(solution)/shard_map/ppermute | solution.py:26
  784.5 20.6 %collective-permute-start.11 = (bf16[2816,128]{1,0:T(8,128)(2,1)S(1)}, bf16[2816,128]{1,0:T(8,128)(2,1)S(1)}, u32[]{:S(2)}, u32[]{:S(2)}) collective-permute-start(bf16[2816,128]{1,0:T(8,128)(2,1)S(1)} %collective-permute-done.10), channel_id=1, source_target_pairs={{2,0},{4,2},{6,4},{8,6},{10,8},{12,10},{14,12},{16,14},{18,16},{20... | collective-permute-start | bytes 2162696 | tf_op jit(solution)/shard_map/ppermute | solution.py:28
  820.5 21.3 %collective-permute-start.12 = (bf16[2816,128]{1,0:T(8,128)(2,1)S(1)}, bf16[2816,128]{1,0:T(8,128)(2,1)}, u32[]{:S(2)}, u32[]{:S(2)}) collective-permute-start(bf16[2816,128]{1,0:T(8,128)(2,1)S(1)} %collective-permute-done.11), channel_id=1, source_target_pairs={{2,0},{4,2},{6,4},{8,6},{10,8},{12,10},{14,12},{16,14},{18,16},{20... | collective-permute-start | bytes 2162696 | tf_op jit(solution)/shard_map/ppermute | solution.py:28
  841.9 31.5 %collective-permute-done.12 = bf16[2816,128]{1,0:T(8,128)(2,1)} collective-permute-done((bf16[2816,128]{1,0:T(8,128)(2,1)S(1)}, bf16[2816,128]{1,0:T(8,128)(2,1)}, u32[]{:S(2)}, u32[]{:S(2)}) %collective-permute-start.12) | collective-permute-done | bytes 720928 | tf_op jit(solution)/shard_map/ppermute | solution.py:28
  873.5 17.4 %collective-permute-start.13 = (bf16[2816,128]{1,0:T(8,128)(2,1)}, bf16[2816,128]{1,0:T(8,128)(2,1)}, u32[]{:S(2)}, u32[]{:S(2)}) collective-permute-start(bf16[2816,128]{1,0:T(8,128)(2,1)} %collective-permute-done.12), channel_id=1, source_target_pairs={{2,0},{4,2},{6,4},{8,6},{10,8},{12,10},{14,12},{16,14},{18,16},{20... | collective-permute-start | bytes 2162696 | tf_op jit(solution)/shard_map/ppermute | solution.py:28
  893.4 23.0 %collective-permute-done.13 = bf16[2816,128]{1,0:T(8,128)(2,1)} collective-permute-done((bf16[2816,128]{1,0:T(8,128)(2,1)}, bf16[2816,128]{1,0:T(8,128)(2,1)}, u32[]{:S(2)}, u32[]{:S(2)}) %collective-permute-start.13) | collective-permute-done | bytes 720928 | tf_op jit(solution)/shard_map/ppermute | solution.py:28
  916.5 24.0 %collective-permute-start.14 = (bf16[2816,128]{1,0:T(8,128)(2,1)}, bf16[2816,128]{1,0:T(8,128)(2,1)}, u32[]{:S(2)}, u32[]{:S(2)}) collective-permute-start(bf16[2816,128]{1,0:T(8,128)(2,1)} %collective-permute-done.13), channel_id=1, source_target_pairs={{2,0},{4,2},{6,4},{8,6},{10,8},{12,10},{14,12},{16,14},{18,16},{20... | collective-permute-start | bytes 2162696 | tf_op jit(solution)/shard_map/ppermute | solution.py:28
  951.9 20.6 %collective-permute-start.15 = (bf16[2816,128]{1,0:T(8,128)(2,1)}, bf16[2816,128]{1,0:T(8,128)(2,1)}, u32[]{:S(2)}, u32[]{:S(2)}) collective-permute-start(bf16[2816,128]{1,0:T(8,128)(2,1)} %collective-permute-done.14), channel_id=1, source_target_pairs={{2,0},{4,2},{6,4},{8,6},{10,8},{12,10},{14,12},{16,14},{18,16},{20... | collective-permute-start | bytes 2162696 | tf_op jit(solution)/shard_map/ppermute | solution.py:28
  1001.7 10.3 gather_fusion
  1012.0 15.1 %copy.92 = bf16[2816,16,128]{0,2,1:T(8,128)(2,1)} copy(bf16[2816,16,128]{2,0,1:T(8,128)(2,1)} %bitcast.222) | data formatting | bytes 23068672 | tf_op jit(solution)/shard_map/transpose | solution.py:16
  1028.5 87.5 %all-gather.11.cloned.1.call-done = bf16[2048,2816]{1,0:T(8,128)(2,1)} async-done(((bf16[128,2816]{1,0:T(8,128)(2,1)}), bf16[2048,2816]{1,0:T(8,128)(2,1)}) %all-gather.11.cloned.1.call-update) | async-done | bytes 11534352 | tf_op jit(solution)/shard_map/all_gather | solution.py:180
  1116.0 14.9 %convolution_convert_fusion.2 = bf16[128,2048]{1,0:T(8,128)(2,1)} fusion(bf16[2816,2048]{0,1:T(8,128)(2,1)} %bitcast.223, bf16[128,2048]{1,0:T(8,128)(2,1)S(1)} %all_gather.19, bf16[2048,2816]{1,0:T(8,128)(2,1)} %all-gather.11.cloned.1.call-done, f32[130,2816]{1,0:T(8,128)} %maximum_convert_fusion, f32[2816]{0:T(1024)S(1)} %get-tuple-element.204, ...), kind=kOutput, calls=%fused_computation.28 | convolution fusion | flops 2957737984 | bytes 28476416 | tf_op jit(solution)/shard_map/dot_general | solution.py:227
  (500 shorter events, 585.5 us)
Async XLA Ops:
  6.5 642.3 %copy-start = (bf16[512,2048]{1,0:T(8,128)(2,1)S(1)}, bf16[512,2048]{1,0:T(8,128)(2,1)}, u32[]{:S(2)}) copy-start(bf16[512,2048]{1,0:T(8,128)(2,1)} %param.27) | copy-start | bytes 6291460
  6.5 587.0 %all-gather.7.cloned.1.call-start = ((), (), s32[]{:S(2)}) async-start(), calls=%async_computation.3 | async-start | bytes 2228224 | tf_op jit(solution)/shard_map/all_gather | solution.py:38
  514.4 125.2 %all-gather.5.cloned.1.call-start = ((), (), s32[]{:S(2)}) async-start(), calls=%async_computation.2 | async-start | bytes 2228224 | tf_op jit(solution)/shard_map/all_gather | solution.py:38
  544.8 347.5 %reduce-scatter.3.cloned.1.call-start = ((), (), s32[]{:S(2)}) async-start(), calls=%async_computation.4 | async-start | bytes 786432 | tf_op jit(solution)/shard_map/reduce_scatter | solution.py:198
  651.1 289.3 %copy-start.38 = (f32[2048]{0:T(1024)S(1)}, f32[2048]{0:T(1024)}, u32[]{:S(2)}) copy-start(f32[2048]{0:T(1024)} %param.29) | copy-start | bytes 24580
  651.1 341.0 %all-gather.9.cloned.1.call-start = ((), (), s32[]{:S(2)}) async-start(), calls=%async_computation.5 | async-start | bytes 12255232 | tf_op jit(solution)/shard_map/all_gather | solution.py:179
  651.7 464.3 %all-gather.11.cloned.1.call-start = ((), (), s32[]{:S(2)}) async-start(), calls=%async_computation.6 | async-start | bytes 12255232 | tf_op jit(solution)/shard_map/all_gather | solution.py:180
  652.3 484.9 %reduce-scatter.5.cloned.1.call-start = ((), (), s32[]{:S(2)}) async-start(), calls=%async_computation.7 | async-start | bytes 786432 | tf_op jit(solution)/shard_map/reduce_scatter | solution.py:226
  652.3 53.0 %collective-permute-start.1 = (bf16[2816,128]{1,0:T(8,128)(2,1)}, bf16[2816,128]{1,0:T(8,128)(2,1)S(1)}, u32[]{:S(2)}, u32[]{:S(2)}) collective-permute-start(bf16[2816,128]{1,0:T(8,128)(2,1)} %param.33), channel_id=1, source_target_pairs={{0,2},{2,4},{4,6},{6,8},{8,10},{10,12},{12,14},{14,16},{16,18},{18... | collective-permute-start | bytes 2162696 | tf_op jit(solution)/shard_map/ppermute | solution.py:26
  705.3 35.4 %collective-permute-start.2 = (bf16[2816,128]{1,0:T(8,128)(2,1)S(1)}, bf16[2816,128]{1,0:T(8,128)(2,1)S(1)}, u32[]{:S(2)}, u32[]{:S(2)}) collective-permute-start(bf16[2816,128]{1,0:T(8,128)(2,1)S(1)} %collective-permute-done.1), channel_id=1, source_target_pairs={{0,2},{2,4},{4,6},{6,8},{8,10},{10,12},{12,14},{14,16},{16,18},{18... | collective-permute-start | bytes 2162696 | tf_op jit(solution)/shard_map/ppermute | solution.py:26
  705.3 35.4 %collective-permute-start.9 = (bf16[2816,128]{1,0:T(8,128)(2,1)}, bf16[2816,128]{1,0:T(8,128)(2,1)S(1)}, u32[]{:S(2)}, u32[]{:S(2)}) collective-permute-start(bf16[2816,128]{1,0:T(8,128)(2,1)} %param.33), channel_id=1, source_target_pairs={{2,0},{4,2},{6,4},{8,6},{10,8},{12,10},{14,12},{16,14},{18,16},{20... | collective-permute-start | bytes 2162696 | tf_op jit(solution)/shard_map/ppermute | solution.py:28
  740.7 41.3 %collective-permute-start.3 = (bf16[2816,128]{1,0:T(8,128)(2,1)S(1)}, bf16[2816,128]{1,0:T(8,128)(2,1)S(1)}, u32[]{:S(2)}, u32[]{:S(2)}) collective-permute-start(bf16[2816,128]{1,0:T(8,128)(2,1)S(1)} %collective-permute-done.2), channel_id=1, source_target_pairs={{0,2},{2,4},{4,6},{6,8},{8,10},{10,12},{12,14},{14,16},{16,18},{18... | collective-permute-start | bytes 2162696 | tf_op jit(solution)/shard_map/ppermute | solution.py:26
  741.6 42.9 %collective-permute-start.10 = (bf16[2816,128]{1,0:T(8,128)(2,1)S(1)}, bf16[2816,128]{1,0:T(8,128)(2,1)S(1)}, u32[]{:S(2)}, u32[]{:S(2)}) collective-permute-start(bf16[2816,128]{1,0:T(8,128)(2,1)S(1)} %collective-permute-done.9), channel_id=1, source_target_pairs={{2,0},{4,2},{6,4},{8,6},{10,8},{12,10},{14,12},{16,14},{18,16},{20... | collective-permute-start | bytes 2162696 | tf_op jit(solution)/shard_map/ppermute | solution.py:28
  782.0 27.7 %collective-permute-start.4 = (bf16[2816,128]{1,0:T(8,128)(2,1)S(1)}, bf16[2816,128]{1,0:T(8,128)(2,1)S(1)}, u32[]{:S(2)}, u32[]{:S(2)}) collective-permute-start(bf16[2816,128]{1,0:T(8,128)(2,1)S(1)} %collective-permute-done.3), channel_id=1, source_target_pairs={{0,2},{2,4},{4,6},{6,8},{8,10},{10,12},{12,14},{14,16},{16,18},{18... | collective-permute-start | bytes 2162696 | tf_op jit(solution)/shard_map/ppermute | solution.py:26
  784.5 36.0 %collective-permute-start.11 = (bf16[2816,128]{1,0:T(8,128)(2,1)S(1)}, bf16[2816,128]{1,0:T(8,128)(2,1)S(1)}, u32[]{:S(2)}, u32[]{:S(2)}) collective-permute-start(bf16[2816,128]{1,0:T(8,128)(2,1)S(1)} %collective-permute-done.10), channel_id=1, source_target_pairs={{2,0},{4,2},{6,4},{8,6},{10,8},{12,10},{14,12},{16,14},{18,16},{20... | collective-permute-start | bytes 2162696 | tf_op jit(solution)/shard_map/ppermute | solution.py:28
  809.8 32.1 %collective-permute-start.5 = (bf16[2816,128]{1,0:T(8,128)(2,1)S(1)}, bf16[2816,128]{1,0:T(8,128)(2,1)S(1)}, u32[]{:S(2)}, u32[]{:S(2)}) collective-permute-start(bf16[2816,128]{1,0:T(8,128)(2,1)S(1)} %collective-permute-done.4), channel_id=1, source_target_pairs={{0,2},{2,4},{4,6},{6,8},{8,10},{10,12},{12,14},{14,16},{16,18},{18... | collective-permute-start | bytes 2162696 | tf_op jit(solution)/shard_map/ppermute | solution.py:26
  820.5 53.0 %collective-permute-start.12 = (bf16[2816,128]{1,0:T(8,128)(2,1)S(1)}, bf16[2816,128]{1,0:T(8,128)(2,1)}, u32[]{:S(2)}, u32[]{:S(2)}) collective-permute-start(bf16[2816,128]{1,0:T(8,128)(2,1)S(1)} %collective-permute-done.11), channel_id=1, source_target_pairs={{2,0},{4,2},{6,4},{8,6},{10,8},{12,10},{14,12},{16,14},{18,16},{20... | collective-permute-start | bytes 2162696 | tf_op jit(solution)/shard_map/ppermute | solution.py:28
  841.8 49.0 %collective-permute-start.6 = (bf16[2816,128]{1,0:T(8,128)(2,1)S(1)}, bf16[2816,128]{1,0:T(8,128)(2,1)}, u32[]{:S(2)}, u32[]{:S(2)}) collective-permute-start(bf16[2816,128]{1,0:T(8,128)(2,1)S(1)} %collective-permute-done.5), channel_id=1, source_target_pairs={{0,2},{2,4},{4,6},{6,8},{8,10},{10,12},{12,14},{14,16},{16,18},{18... | collective-permute-start | bytes 2162696 | tf_op jit(solution)/shard_map/ppermute | solution.py:26
  873.5 43.0 %collective-permute-start.13 = (bf16[2816,128]{1,0:T(8,128)(2,1)}, bf16[2816,128]{1,0:T(8,128)(2,1)}, u32[]{:S(2)}, u32[]{:S(2)}) collective-permute-start(bf16[2816,128]{1,0:T(8,128)(2,1)} %collective-permute-done.12), channel_id=1, source_target_pairs={{2,0},{4,2},{6,4},{8,6},{10,8},{12,10},{14,12},{16,14},{18,16},{20... | collective-permute-start | bytes 2162696 | tf_op jit(solution)/shard_map/ppermute | solution.py:28
  890.9 49.6 %collective-permute-start.7 = (bf16[2816,128]{1,0:T(8,128)(2,1)}, bf16[2816,128]{1,0:T(8,128)(2,1)}, u32[]{:S(2)}, u32[]{:S(2)}) collective-permute-start(bf16[2816,128]{1,0:T(8,128)(2,1)} %collective-permute-done.6), channel_id=1, source_target_pairs={{0,2},{2,4},{4,6},{6,8},{8,10},{10,12},{12,14},{14,16},{16,18},{18... | collective-permute-start | bytes 2162696 | tf_op jit(solution)/shard_map/ppermute | solution.py:26
  916.5 35.4 %collective-permute-start.14 = (bf16[2816,128]{1,0:T(8,128)(2,1)}, bf16[2816,128]{1,0:T(8,128)(2,1)}, u32[]{:S(2)}, u32[]{:S(2)}) collective-permute-start(bf16[2816,128]{1,0:T(8,128)(2,1)} %collective-permute-done.13), channel_id=1, source_target_pairs={{2,0},{4,2},{6,4},{8,6},{10,8},{12,10},{14,12},{16,14},{18,16},{20... | collective-permute-start | bytes 2162696 | tf_op jit(solution)/shard_map/ppermute | solution.py:28
  940.4 32.0 %collective-permute-start.8 = (bf16[2816,128]{1,0:T(8,128)(2,1)}, bf16[2816,128]{1,0:T(8,128)(2,1)S(1)}, u32[]{:S(2)}, u32[]{:S(2)}) collective-permute-start(bf16[2816,128]{1,0:T(8,128)(2,1)} %collective-permute-done.7), channel_id=1, source_target_pairs={{0,2},{2,4},{4,6},{6,8},{8,10},{10,12},{12,14},{14,16},{16,18},{18... | collective-permute-start | bytes 2162696 | tf_op jit(solution)/shard_map/ppermute | solution.py:26
  951.9 47.8 %collective-permute-start.15 = (bf16[2816,128]{1,0:T(8,128)(2,1)}, bf16[2816,128]{1,0:T(8,128)(2,1)}, u32[]{:S(2)}, u32[]{:S(2)}) collective-permute-start(bf16[2816,128]{1,0:T(8,128)(2,1)} %collective-permute-done.14), channel_id=1, source_target_pairs={{2,0},{4,2},{6,4},{8,6},{10,8},{12,10},{14,12},{16,14},{18,16},{20... | collective-permute-start | bytes 2162696 | tf_op jit(solution)/shard_map/ppermute | solution.py:28
  998.2 29.0 %collective-permute-start = (bf16[2,2816]{1,0:T(2,128)(2,1)S(1)}, bf16[2,2816]{1,0:T(2,128)(2,1)S(1)}, u32[]{:S(2)}, u32[]{:S(2)}) collective-permute-start(bf16[2,2816]{1,0:T(2,128)(2,1)S(1)} %slice.168), channel_id=1, source_target_pairs={{0,2},{2,4},{4,6},{6,8},{8,10},{10,12},{12,14},{14,16},{16,18},{18... | collective-permute-start | bytes 33800 | tf_op jit(solution)/shard_map/ppermute | solution.py:58
  (99 other events, 1009.9 us)
Sparse Core Ops, SparseCore 0:
  514.5 63.0 all-gather.6
  580.4 59.1 all-gather.4
  651.2 41.1 reduce-scatter.2
  695.1 254.1 all-gather.8
  951.9 164.0 all-gather.10
  1131.0 6.0 reduce-scatter.4
